TPU v7x, 32 devices: a whole 2x2x4 slice. The times are simulated.
32 devices in a mesh: kv: 8 (over z, y), tp: 4 (over x, core).
Axes of the slice: x: 2, y: 2, z: 4, core: 2. Of those that a mesh axis runs over, the one named last changes fastest.
Arguments:
- tokens: bfloat16 [128, 4096], P('kv'), may hold values from -6 to 6
- dec_tokens: bfloat16 [8, 4096], P('kv'), may hold values from -6 to 6
- norm_gain: float32 [4096], replicated, may hold values from 0.1 to 1.9
- w_query: bfloat16 [2, 4096, 1024], P(None, None, 'tp'), may hold values from -0.09375 to 0.09375
- w_key: bfloat16 [2, 4096, 1024], P(None, None, 'tp'), may hold values from -0.15625 to 0.15625
- w_value: bfloat16 [4096, 2048], P(None, 'tp'), may hold values from -0.09375 to 0.09375
- w_out: bfloat16 [2048, 4096], P('tp'), may hold values from -0.125 to 0.125
- head_gain: float32 [256], replicated, may hold values from 0.1 to 1.9
- mix_lambda: float32 [8], P('tp'), may hold values from 0.3 to 0.8
- ctx_keys: bfloat16 [2, 8192, 1024], P(None, 'kv', 'tp'), may hold values from -600 to 600
- ctx_values: bfloat16 [8192, 2048], P('kv', 'tp'), may hold values from -6 to 6
- dec_keys: bfloat16 [2, 8, 2048, 1024], P(None, 'kv', None, 'tp'), may hold values from -600 to 600
- dec_values: bfloat16 [8, 2048, 2048], P('kv', None, 'tp'), may hold values from -6 to 6
- dec_len: int32 [8], P('kv'), may hold values from 256 to 2048, as said below
Outputs:
- piece_out: bfloat16 [128, 4096], P('kv', 'tp')
- dec_out: bfloat16 [8, 4096], P('kv', 'tp')
Inputs may be any that keep to these rules, and one draw needn't show every extreme that they name: `dec_len`: some decoding sequence has exactly 2048 cached positions.
All inputs are finite; a program needn't handle non-finite values.
Results may differ from a plain program's by a relative error of at most 0.03.
The roundings to bfloat16 on the way count: a program that leaves them out, or rounds other values in their place, can miss the bound.
Values may be sent and summed in bfloat16 or wider, within the bound.
A program may use at most 64 MiB of HBM per device.

v0:
```python
import math

import jax
import jax.numpy as jnp
from jax import lax
from jax.sharding import PartitionSpec as P

DH = 128


epsilon = 1e-06


def map_scores(block, ctx_keys, own_keys, block_pos, own_pos, cols, scale):
    pairs = []
    for part in range(2):
        query = block[:, part, cols]
        far = (
            jnp.einsum(
                "nd,md->nm", query, ctx_keys[part][:, cols], preferred_element_type=jnp.float32
            )
            * scale
        )
        near = (
            jnp.einsum(
                "nd,md->nm", query, own_keys[:, part, cols], preferred_element_type=jnp.float32
            )
            * scale
        )
        near = jnp.where(own_pos[None, :] <= block_pos[:, None], near, -jnp.inf)
        pairs.append((far, near))
    return pairs


def body(
    tokens,
    dec_tokens,
    norm_gain,
    w_query,
    w_key,
    w_value,
    w_out,
    head_gain,
    mix_lambda,
    ctx_keys,
    ctx_values,
    dec_keys,
    dec_values,
    dec_len,
):
    scale = DH ** (-0.5)
    local_heads = mix_lambda.shape[0]
    piece_rows = tokens.shape[0]
    dec_rows = dec_tokens.shape[0]
    rows = jnp.concatenate([tokens, dec_tokens], axis=0)
    xf = rows.astype(jnp.float32)
    normed = (
        xf * lax.rsqrt(jnp.mean(xf * xf, axis=-1, keepdims=True) + epsilon) * norm_gain
    ).astype(jnp.bfloat16)
    query = jnp.einsum("rd,cdn->rcn", normed, w_query, preferred_element_type=jnp.float32).astype(
        jnp.bfloat16
    )
    keys = jnp.einsum("rd,cdn->rcn", normed, w_key, preferred_element_type=jnp.float32).astype(
        jnp.bfloat16
    )
    value = jnp.dot(normed, w_value, preferred_element_type=jnp.float32).astype(jnp.bfloat16)
    own_keys = keys[:piece_rows]
    own_values = value[:piece_rows]
    own_pos = lax.axis_index("kv") * piece_rows + jnp.arange(piece_rows, dtype=jnp.int32)
    gathered = lax.all_gather(query[:piece_rows], "kv", axis=0, tiled=True)
    total_rows = gathered.shape[0]
    width = gathered.shape[2]
    block = math.gcd(total_rows, 512)
    blocks = total_rows // block
    query_blocks = gathered.reshape(blocks, block, 2, width)
    pos_blocks = jnp.arange(total_rows, dtype=jnp.int32).reshape(blocks, block)

    def block_stats(args):
        qb, qpos = args
        maxima, totals = ([], [])
        for head in range(local_heads):
            cols = slice(head * DH, (head + 1) * DH)
            for far, near in map_scores(qb, ctx_keys, own_keys, qpos, own_pos, cols, scale):
                top = jnp.maximum(jnp.max(far, axis=-1), jnp.max(near, axis=-1))
                maxima.append(top)
                totals.append(
                    jnp.sum(jnp.exp(far - top[:, None]), axis=-1)
                    + jnp.sum(jnp.exp(near - top[:, None]), axis=-1)
                )
        return (jnp.stack(maxima), jnp.stack(totals))

    local_max, local_tot = lax.map(block_stats, (query_blocks, pos_blocks))
    local_max = jnp.moveaxis(local_max, 0, 1).reshape(2 * local_heads, total_rows)
    local_tot = jnp.moveaxis(local_tot, 0, 1).reshape(2 * local_heads, total_rows)
    row_top = lax.pmax(local_max, "kv")
    row_sum = lax.psum(local_tot * jnp.exp(local_max - row_top), "kv")

    def block_terms(qb, qpos, top_b, sum_b):
        outputs = []
        for head in range(local_heads):
            cols = slice(head * DH, (head + 1) * DH)
            vcols = slice(head * 2 * DH, (head + 1) * 2 * DH)
            pairs = map_scores(qb, ctx_keys, own_keys, qpos, own_pos, cols, scale)
            shares = []
            for part in range(2):
                far, near = pairs[part]
                top = top_b[2 * head + part][:, None]
                denom = sum_b[2 * head + part][:, None]
                shares.append((jnp.exp(far - top) / denom, jnp.exp(near - top) / denom))
            lam = mix_lambda[head]
            far_w = (shares[0][0] - lam * shares[1][0]).astype(jnp.bfloat16)
            near_w = (shares[0][1] - lam * shares[1][1]).astype(jnp.bfloat16)
            outputs.append(
                jnp.dot(far_w, ctx_values[:, vcols], preferred_element_type=jnp.float32)
                + jnp.dot(near_w, own_values[:, vcols], preferred_element_type=jnp.float32)
            )
        return jnp.concatenate(outputs, axis=-1)

    top_blocks = jnp.moveaxis(row_top.reshape(2 * local_heads, blocks, block), 1, 0)
    sum_blocks = jnp.moveaxis(row_sum.reshape(2 * local_heads, blocks, block), 1, 0)
    terms = lax.map(
        lambda args: block_terms(*args), (query_blocks, pos_blocks, top_blocks, sum_blocks)
    )
    piece_att = lax.psum_scatter(
        terms.reshape(total_rows, terms.shape[2]), "kv", scatter_dimension=0, tiled=True
    )
    dec_query = query[piece_rows:].reshape(dec_rows, 2, local_heads, DH)
    dec_new_k = keys[piece_rows:].reshape(dec_rows, 2, local_heads, DH)
    dec_new_v = value[piece_rows:].reshape(dec_rows, local_heads, 2 * DH)
    slots = dec_keys.shape[2]
    cache_k = dec_keys.reshape(2, dec_rows, slots, local_heads, DH)
    far = (
        jnp.einsum("bchd,cbjhd->bchj", dec_query, cache_k, preferred_element_type=jnp.float32)
        * scale
    )
    valid = jnp.arange(slots, dtype=jnp.int32)[None, :] < dec_len[:, None]
    far = jnp.where(valid[:, None, None, :], far, -jnp.inf)
    near = (
        jnp.einsum("bchd,bchd->bch", dec_query, dec_new_k, preferred_element_type=jnp.float32)
        * scale
    )
    top = jnp.maximum(jnp.max(far, axis=-1), near)
    denom = jnp.sum(jnp.exp(far - top[..., None]), axis=-1) + jnp.exp(near - top)
    far_p = jnp.exp(far - top[..., None]) / denom[..., None]
    near_p = jnp.exp(near - top) / denom
    far_w = (far_p[:, 0] - mix_lambda[None, :, None] * far_p[:, 1]).astype(jnp.bfloat16)
    near_w = (near_p[:, 0] - mix_lambda[None, :] * near_p[:, 1]).astype(jnp.bfloat16)
    cache_v = dec_values.reshape(dec_rows, slots, local_heads, 2 * DH)
    dec_att = jnp.einsum("bhj,bjhe->bhe", far_w, cache_v, preferred_element_type=jnp.float32)
    dec_att = dec_att + near_w.astype(jnp.float32)[..., None] * dec_new_v.astype(jnp.float32)
    attended = jnp.concatenate(
        [piece_att.reshape(piece_rows, local_heads, 2 * DH), dec_att], axis=0
    )
    heads_out = (
        attended
        * lax.rsqrt(jnp.mean(attended * attended, axis=-1, keepdims=True) + epsilon)
        * head_gain
    )
    heads_out = heads_out.astype(jnp.bfloat16).reshape(piece_rows + dec_rows, local_heads * 2 * DH)
    partial_value = jnp.dot(heads_out, w_out, preferred_element_type=jnp.float32)
    partial_value = lax.optimization_barrier(partial_value.astype(jnp.bfloat16)).astype(jnp.float32)
    summed = lax.psum_scatter(
        partial_value.astype(jnp.bfloat16), "tp", scatter_dimension=1, tiled=True
    )
    return (summed[:piece_rows], summed[piece_rows:])


def solution(mesh):
    in_specs = (
        P("kv", None),
        P("kv", None),
        P(),
        P(None, None, "tp"),
        P(None, None, "tp"),
        P(None, "tp"),
        P("tp", None),
        P(),
        P("tp"),
        P(None, "kv", "tp"),
        P("kv", "tp"),
        P(None, "kv", None, "tp"),
        P("kv", None, "tp"),
        P("kv"),
    )
    out_specs = (P("kv", "tp"), P("kv", "tp"))
    return jax.shard_map(body, mesh=mesh, in_specs=in_specs, out_specs=out_specs, check_vma=False)
```

profile of v0, /device:TPU:0, one launch (start us, length us, event | category | flops | bytes accessed | tf_op | source)
XLA Modules:
  0.0 190.0 jit_solution(14455661820327340171)
XLA Ops:
  7.3 1.2 fusion.8
  8.5 3.1 %convolution_convert_fusion.3 = bf16[17,2,256]{2,0,1:T(8,128)(2,1)S(1)} fusion(bf16[2,4096,256]{2,1,0:T(8,128)(2,1)} %param.17, f32[4096]{0:T(1024)} %param.16, f32[17]{0:T(128)S(1)} %add_rsqrt_fusion.1, bf16[1,4096]{1,0:T(2,128)(2,1)} %param.15, bf16[16,4096]{1,0:T(8,128)(2,1)} %param.14), kind=kOutput, calls=%fused_computation.11 | convolution fusion | flops 71799296 | bytes 4367428 | tf_op jit(solution)/shard_map/rd,cdn->rcn/dot_general | solution.py:60
  11.6 32.3 %all_gather.3 = bf16[128,2,256]{2,0,1:T(8,128)(2,1)S(1)} all-gather(bf16[16,2,256]{2,0,1:T(8,128)(2,1)S(1)} %slice.222), channel_id=1, replica_groups=mesh['kv'=8,'tp'=4] {'kv'}, dimensions={0}, use_global_device_ids=true | all-gather | bytes 147456 | tf_op jit(solution)/shard_map/all_gather | solution.py:70
  44.0 0.7 convolution_convert_fusion.2
  46.1 0.3 fusion.64
  47.9 21.4 %pmax.7 = f32[4,128]{1,0:T(4,128)S(1)} all-reduce(f32[4,128]{1,0:T(4,128)S(1)} %pad_maximum_fusion.2), channel_id=1, replica_groups=mesh['kv'=8,'tp'=4] {'kv'}, use_global_device_ids=true, to_apply=%region_9.10 | all-reduce | flops 512 | bytes 4096 | tf_op jit(solution)/shard_map/pmax | solution.py:95
  69.3 17.1 %psum.7 = f32[4,128]{1,0:T(4,128)S(1)} all-reduce(f32[4,128]{1,0:T(4,128)S(1)} %maximum_multiply_fusion.2), channel_id=1, replica_groups=mesh['kv'=8,'tp'=4] {'kv'}, use_global_device_ids=true, to_apply=%region_18.19 | all-reduce | flops 512 | bytes 4096 | tf_op jit(solution)/shard_map/psum | solution.py:96
  86.4 3.0 %convolution_convert_fusion.1 = bf16[17,512]{1,0:T(8,128)(2,1)S(1)} fusion(bf16[4096,512]{1,0:T(8,128)(2,1)} %param.19, f32[4096]{0:T(1024)S(1)} %copy-done.5, f32[17]{0:T(128)S(1)} %add_rsqrt_fusion.1, bf16[1,4096]{1,0:T(2,128)(2,1)S(1)} %copy-done.4, bf16[16,4096]{1,0:T(8,128)(2,1)S(1)} %copy-done.2), kind=kOutput, calls=%fused_computation.9 | convolution fusion | flops 71799296 | bytes 4367428 | tf_op jit(solution)/shard_map/dot_general | solution.py:66
  89.4 0.6 fusion.57
  90.0 0.8 fusion.30
  90.8 2.1 %convolution_add_fusion.1 = f32[128,256]{1,0:T(8,128)S(1)} fusion(f32[128,256]{1,0:T(8,128)S(1)} %fusion.30, bf16[1024,512]{1,0:T(8,128)(2,1)} %param.24, f32[128,1024]{1,0:T(8,128)S(1)} %get-tuple-element.85, f32[128,1024]{1,0:T(8,128)S(1)} %get-tuple-element.89, f32[128]{0:T(128)S(1)} %get-tuple-element.61, f32[128]{0:T(128)S(1)} %get-tuple-element.57, ...), kind=kOutput, calls=%fused_computation.8 | convolution fusion | flops 68059136 | bytes 1837568 | tf_op jit(solution)/shard_map/while/body/eval_jaxpr/dot_general | solution.py:114
  92.9 0.9 fusion.28
  93.8 1.0 convolution_add_fusion
  94.8 0.7 pad_maximum_fusion
  95.7 2.9 %copy.25 = bf16[2,1,2048,256]{2,3,0,1:T(8,128)(2,1)S(1)} copy(bf16[2,1,2048,256]{3,2,1,0:T(8,128)(2,1)} %param.25) | data formatting | bytes 4194304 | tf_op jit(solution)/shard_map/reshape.28
  98.7 0.4 fusion.45
  100.3 2.6 %reshape.276 = bf16[2048,2,256]{2,1,0:T(2,128)(2,1)S(1)} reshape(bf16[1,2048,512]{2,1,0:T(8,128)(2,1)} %param.26) | data formatting | bytes 4194304 | tf_op jit(solution)/shard_map/reshape.37
  102.9 0.4 fusion
  103.4 53.5 %reduce-scatter.3.cloned.1.call-done = f32[16,512]{1,0:T(8,128)} async-done(((f32[128,512]{1,0:T(8,128)}), f32[16,512]{1,0:T(8,128)}) %reduce-scatter.3.cloned.1.call-update) | async-done | bytes 32784 | tf_op jit(solution)/shard_map/reduce_scatter | solution.py:124
  156.9 0.8 reshape.277
  157.9 3.6 %convolution_convert_fusion = bf16[17,4096]{1,0:T(8,128)(2,1)} fusion(bf16[512,4096]{1,0:T(8,128)(2,1)} %param.20, f32[17,512]{1,0:T(8,128)S(1)} %bitcast.157, f32[1,512]{1,0:T(1,128)S(1)} %bitcast.161, f32[16,512]{1,0:T(8,128)} %reduce-scatter.3.cloned.1.call-done, f32[512]{0:T(512)S(1)} %bitcast.162), kind=kOutput, calls=%fused_computation | convolution fusion | flops 71407616 | bytes 4405248 | tf_op jit(solution)/shard_map/dot_general | solution.py:160
  161.5 19.0 %reduce-scatter.5.cloned.1.call-done = bf16[17,1024]{1,0:T(8,128)(2,1)} async-done(((bf16[17,4096]{1,0:T(8,128)(2,1)}), bf16[17,1024]{1,0:T(8,128)(2,1)}) %reduce-scatter.5.cloned.1.call-update) | async-done | bytes 34832 | tf_op jit(solution)/shard_map/reduce_scatter | solution.py:162
  180.5 1.4 slice.242
  181.8 1.3 slice.243
  (73 shorter events, 3.9 us)
Async XLA Ops:
  7.2 96.2 %copy-start = (f32[256]{0:T(256)S(1)}, f32[256]{0:T(256)}, u32[]{:S(2)}) copy-start(f32[256]{0:T(256)} %param.21) | copy-start | bytes 3076
  7.2 36.8 %copy-start.2 = (bf16[16,4096]{1,0:T(8,128)(2,1)S(1)}, bf16[16,4096]{1,0:T(8,128)(2,1)}, u32[]{:S(2)}) copy-start(bf16[16,4096]{1,0:T(8,128)(2,1)} %param.14) | copy-start | bytes 393220
  7.2 36.8 %copy-start.4 = (bf16[1,4096]{1,0:T(2,128)(2,1)S(1)}, bf16[1,4096]{1,0:T(2,128)(2,1)}, u32[]{:S(2)}) copy-start(bf16[1,4096]{1,0:T(2,128)(2,1)} %param.15) | copy-start | bytes 24580
  7.2 36.8 %copy-start.5 = (f32[4096]{0:T(1024)S(1)}, f32[4096]{0:T(1024)}, u32[]{:S(2)}) copy-start(f32[4096]{0:T(1024)} %param.16) | copy-start | bytes 49156
  7.2 149.7 %reduce-scatter.3.cloned.1.call-start = ((), (), s32[]{:S(2)}) async-start(), calls=%async_computation.2 | async-start | bytes 294912 | tf_op jit(solution)/shard_map/reduce_scatter | solution.py:124
  7.3 36.7 %copy-start.1 = (bf16[2,4096,256]{2,1,0:T(8,128)(2,1)S(1)}, bf16[2,4096,256]{2,1,0:T(8,128)(2,1)}, u32[]{:S(2)}) copy-start(bf16[2,4096,256]{2,1,0:T(8,128)(2,1)} %param.18) | copy-start | bytes 12582916
  8.5 36.7 %copy-start.3 = (bf16[2,1024,256]{2,1,0:T(8,128)(2,1)S(1)}, bf16[2,1024,256]{2,1,0:T(8,128)(2,1)}, u32[]{:S(2)}) copy-start(bf16[2,1024,256]{2,1,0:T(8,128)(2,1)} %param.23) | copy-start | bytes 3145732
  45.9 43.4 %copy-start.6 = (f32[2]{0:T(128)S(1)}, f32[2]{0:T(128)}, u32[]{:S(2)}) copy-start(f32[2]{0:T(128)} %param.22) | copy-start | bytes 28
  86.4 7.4 %copy-start.7 = (bf16[1024,512]{1,0:T(8,128)(2,1)S(1)}, bf16[1024,512]{1,0:T(8,128)(2,1)}, u32[]{:S(2)}) copy-start(bf16[1024,512]{1,0:T(8,128)(2,1)} %param.24) | copy-start | bytes 3145732
  95.6 84.9 %reduce-scatter.5.cloned.1.call-start = ((), (), s32[]{:S(2)}) async-start(), calls=%async_computation.3 | async-start | bytes 245760 | tf_op jit(solution)/shard_map/reduce_scatter | solution.py:162
Sparse Core Ops, SparseCore 0:
  95.7 61.1 reduce-scatter.2
  161.6 18.8 reduce-scatter.4
where the time goes:
time: 191 us; the launch traced here: 190 us
  waiting for transfers between devices  72.5 us (38%)
  blocking collectives  70.8 us (37%)
  matrix products  17.9 us (9%)
  between operations  15 us (8%)
  local copies, waits for them, and re-layouts  9.9 us (5%)
  other arithmetic  3.85 us (2%)
    reduce_scatter x1, waiting for transfers between devices, body(): lax.psum_scatter(terms.reshape(total_rows, terms.shape[2]), 'kv', scatter...  53.5 us
    all_gather x1, blocking collectives, body(): gathered = lax.all_gather(query[:piece_rows], 'kv', axis=0, tiled=True)  32.3 us
    pmax x1, blocking collectives, body(): row_top = lax.pmax(local_max, 'kv')  21.4 us
    reduce_scatter x1, waiting for transfers between devices, body(): lax.psum_scatter(partial_value.astype(jnp.bfloat16), 'tp', scatter_dimens...  19 us
    psum x1, blocking collectives, body(): row_sum = lax.psum(local_tot * jnp.exp(local_max - row_top), 'kv')  17.1 us
    another operation x4, local copies, waits for them, and re-layouts  5.52 us
  transfers between devices with their start and end apart: 2, of which 2 were waited for; matrix products, arithmetic and copies ran while one was open for 4% of the time, Pallas kernels for 0%

commit v1 on v0

v1 whole, which is shorter than its diff:
```python
import functools
import math

import jax
import jax.numpy as jnp
from jax import lax
from jax.experimental import pallas as pl
from jax.experimental.pallas import tpu as pltpu
from jax.sharding import PartitionSpec as P

DH = 128
epsilon = 1e-06
MESH = pl.DeviceIdType.MESH
F32 = jnp.float32
BF16 = jnp.bfloat16
LANES = 128
C_EXP = DH ** (-0.5) * math.log2(math.e)


def dot(a, b):
    return jnp.dot(a, b, preferred_element_type=F32)


def dot_nt(a, b):
    return lax.dot_general(a, b, (((1,), (1,)), ((), ())), preferred_element_type=F32)


def kernel(
    kv, tp,
    tokens, dec_tokens, norm_gain, w_query, w_key, w_value, w_out, head_gain,
    mix_lambda, dec_len, ctx_keys, ctx_values, dec_keys, dec_values,
    piece_out, dec_out,
    tok_v, dtok_v, gain_v, hgain_v, wq_v, wk_v, wv_v, wo_v,
    ck_v, cv_v, dk_v, dv_v,
    xs, q_all, kown, vown, e_v, st_all, att_send, att_recv, p_send, p_recv, d_send, d_recv,
    sem_small, sem_q, sem_k, sem_v, sem_o, sem_c, sem_d,
    qs_sem, qr_sem, ss_sem, sr_sem, as_sem, ar_sem, ps_sem, pr_sem, ds_sem, dr_sem,
):
    me = lax.axis_index("kv")
    mt = lax.axis_index("tp")
    rows, width = tokens.shape
    drows = dec_tokens.shape[0]
    w = w_query.shape[2]
    heads = w // DH
    ctx = ctx_keys.shape[1]
    slots = dec_keys.shape[2]
    total = rows * kv
    cols = w_out.shape[1] // tp
    blocks = total // LANES
    padded = xs.shape[0]

    small = [
        pltpu.make_async_copy(tokens, tok_v, sem_small.at[0]),
        pltpu.make_async_copy(dec_tokens, dtok_v, sem_small.at[1]),
        pltpu.make_async_copy(norm_gain, gain_v, sem_small.at[2]),
        pltpu.make_async_copy(head_gain, hgain_v, sem_small.at[3]),
    ]
    for c in small:
        c.start()

    def weight_copies(src, dst, sem, parts):
        step = width // parts
        out = []
        for c in range(2):
            row = []
            for i in range(parts):
                sl = pl.ds(i * step, step)
                row.append(
                    pltpu.make_async_copy(src.at[c, sl], dst.at[c, sl], sem.at[c * parts + i])
                )
            out.append(row)
        return out

    parts = 2
    q_copies = weight_copies(w_query, wq_v, sem_q, parts)
    k_copies = weight_copies(w_key, wk_v, sem_k, parts)
    vstep = width // 4
    v_copies = [
        pltpu.make_async_copy(
            w_value.at[pl.ds(i * vstep, vstep)], wv_v.at[pl.ds(i * vstep, vstep)], sem_v.at[i]
        )
        for i in range(4)
    ]
    ck_copies = [pltpu.make_async_copy(ctx_keys.at[c], ck_v.at[c], sem_c.at[c]) for c in range(2)]
    cv_copy = pltpu.make_async_copy(ctx_values, cv_v, sem_c.at[2])
    dk_copies = [pltpu.make_async_copy(dec_keys.at[c], dk_v.at[c], sem_d.at[c]) for c in range(2)]
    dv_copy = pltpu.make_async_copy(dec_values, dv_v, sem_d.at[2])
    wo_copies = []
    for d in range(tp):
        t = lax.rem(mt + d, tp)
        start = pl.multiple_of(t * cols, LANES)
        wo_copies.append(
            pltpu.make_async_copy(w_out.at[:, pl.ds(start, cols)], wo_v.at[d], sem_o.at[d])
        )
    for row in q_copies + k_copies:
        for c in row:
            c.start()
    for c in v_copies + dk_copies + ck_copies + [cv_copy, dv_copy] + wo_copies:
        c.start()

    barrier = pltpu.get_barrier_semaphore()
    for d in range(1, kv):
        pl.semaphore_signal(
            barrier, inc=1, device_id=(lax.rem(me + d, kv), mt), device_id_type=MESH
        )
    for d in range(1, tp):
        pl.semaphore_signal(
            barrier, inc=1, device_id=(me, lax.rem(mt + d, tp)), device_id_type=MESH
        )

    kown[...] = jnp.zeros_like(kown)
    vown[...] = jnp.zeros_like(vown)
    xs[rows:, :] = jnp.zeros((padded - rows, width), BF16)
    for c in small:
        c.wait()
    gain = gain_v[...]

    def normed(x):
        xf = x.astype(F32)
        inv = lax.rsqrt(jnp.mean(xf * xf, axis=-1, keepdims=True) + epsilon)
        return (xf * inv * gain).astype(BF16)

    xs[0:rows, :] = normed(tok_v[...])
    xs[rows : rows + drows, :] = normed(dtok_v[...])

    def project(copies, weights, c):
        step = width // parts
        acc = None
        for i in range(parts):
            copies[c][i].wait()
            term = dot(xs[:, i * step : (i + 1) * step], weights[c, i * step : (i + 1) * step, :])
            acc = term if acc is None else acc + term
        return acc.astype(BF16)

    dec_q = []
    for c in range(2):
        qc = project(q_copies, wq_v, c)
        q_all[me, :, c * w : (c + 1) * w] = qc[0:rows]
        dec_q.append(qc[rows:])
    pl.semaphore_wait(barrier, kv + tp - 2)

    def to_kv(src, dst, send, recv, d):
        return pltpu.make_async_remote_copy(
            src_ref=src, dst_ref=dst, send_sem=send.at[d], recv_sem=recv.at[d],
            device_id=(lax.rem(me + d, kv), mt), device_id_type=MESH,
        )

    q_sends = [to_kv(q_all.at[me], q_all.at[me], qs_sem, qr_sem, d) for d in range(1, kv)]
    for c in q_sends:
        c.start()

    dec_k = []
    for c in range(2):
        kc = project(k_copies, wk_v, c)
        kown[c, 0:rows, :] = kc[0:rows]
        dec_k.append(kc[rows:])
    acc = None
    for i in range(4):
        v_copies[i].wait()
        term = dot(xs[:, i * vstep : (i + 1) * vstep], wv_v[i * vstep : (i + 1) * vstep, :])
        acc = term if acc is None else acc + term
    vc = acc.astype(BF16)
    vown[0:rows, :] = vc[0:rows]
    dec_v = vc[rows:]

    group = 16
    hrow = lax.broadcasted_iota(jnp.int32, (group, w), 0)
    hcol = lax.broadcasted_iota(jnp.int32, (group, w), 1) // DH
    own_head = hrow == hcol
    row1 = lax.broadcasted_iota(jnp.int32, (group, 1), 0)
    lam_col = jnp.zeros((group, 1), F32)
    for h in range(heads):
        lam_col = jnp.where(row1 == h, mix_lambda[h], lam_col)
    for c in dk_copies:
        c.wait()
    slot_id = lax.broadcasted_iota(jnp.int32, (group, slots), 1)
    dec_far = []
    dec_near = []
    for r in range(drows):
        far_p = []
        near_p = []
        for c in range(2):
            qr = jnp.broadcast_to(dec_q[c][r : r + 1].astype(F32), (group, w))
            qr = jnp.where(own_head, qr, 0.0)
            kr = dec_k[c][r : r + 1].astype(F32)
            near = jnp.sum(qr * kr, axis=-1, keepdims=True)
            far = dot_nt(qr.astype(BF16), dk_v[c, r])
            far = jnp.where(slot_id < dec_len[r], far, -jnp.inf)
            top = jnp.maximum(jnp.max(far, axis=-1, keepdims=True), near)
            ef = jnp.exp2((far - top) * C_EXP)
            en = jnp.exp2((near - top) * C_EXP)
            den = jnp.sum(ef, axis=-1, keepdims=True) + en
            far_p.append(ef / den)
            near_p.append(en / den)
        dec_far.append((far_p[0] - lam_col * far_p[1]).astype(BF16))
        dec_near.append((near_p[0] - lam_col * near_p[1]).astype(BF16).astype(F32))

    for c in ck_copies:
        c.wait()
    for d, c in enumerate(q_sends, 1):
        c.wait_recv()
    nstat = 2 * heads
    srows = st_all.shape[1]

    def score_block(b):
        slot0 = b * (LANES // rows)
        qb = q_all[pl.ds(slot0, LANES // rows)].reshape(LANES, 2 * w)
        pos = b * LANES + lax.broadcasted_iota(jnp.int32, (LANES, LANES), 0)
        key = lax.broadcasted_iota(jnp.int32, (LANES, LANES), 1)
        ok = (key < rows) & (key + me * rows <= pos)
        lane = key
        stats = jnp.zeros((LANES, LANES), F32)
        for h in range(heads):
            for c in range(2):
                q = qb[:, c * w + h * DH : c * w + (h + 1) * DH]
                hs = slice(h * DH, (h + 1) * DH)
                far = dot_nt(q, ck_v[c, :, hs])
                near = dot_nt(q, kown[c, :, hs])
                near = jnp.where(ok, near, -jnp.inf)
                top = jnp.maximum(
                    jnp.max(far, axis=-1, keepdims=True), jnp.max(near, axis=-1, keepdims=True)
                )
                ef = jnp.exp2((far - top) * C_EXP)
                en = jnp.exp2((near - top) * C_EXP)
                tot = jnp.sum(ef, axis=-1, keepdims=True) + jnp.sum(en, axis=-1, keepdims=True)
                i = 2 * h + c
                rs = pl.ds(b * LANES, LANES)
                e_v[i, rs, 0:ctx] = ef
                e_v[i, rs, ctx:] = en
                stats = jnp.where(lane == i, top, stats)
                stats = jnp.where(lane == nstat + i, tot, stats)
        st_all[me, :, pl.ds(pl.multiple_of(b * LANES, LANES), LANES)] = stats.T[0:srows]

    def each_block(f):
        if blocks == 1:
            f(0)
        else:
            pl.loop(0, blocks)(f)

    each_block(score_block)
    st_sends = [to_kv(st_all.at[me], st_all.at[me], ss_sem, sr_sem, d) for d in range(1, kv)]
    for c in st_sends:
        c.start()

    vw = 2 * DH
    hgain = hgain_v[...]
    dv_copy.wait()
    vrow = lax.broadcasted_iota(jnp.int32, (group, heads * vw), 0)
    vcol = lax.broadcasted_iota(jnp.int32, (group, heads * vw), 1) // vw

    def head_norm(att):
        out = []
        for h in range(heads):
            a = att[:, h * vw : (h + 1) * vw]
            inv = lax.rsqrt(jnp.mean(a * a, axis=-1, keepdims=True) + epsilon)
            out.append((a * inv * hgain).astype(BF16))
        return out

    def out_project(ho, d):
        acc = None
        for h in range(heads):
            term = dot(ho[h], wo_v[d, h * vw : (h + 1) * vw, :])
            acc = term if acc is None else acc + term
        return acc.astype(BF16)

    def to_tp(src, dst, send, recv, d):
        return pltpu.make_async_remote_copy(
            src_ref=src.at[d], dst_ref=dst.at[d], send_sem=send.at[d], recv_sem=recv.at[d],
            device_id=(me, lax.rem(mt + d, tp)), device_id_type=MESH,
        )

    dec_att = []
    for r in range(drows):
        att = dot(dec_far[r], dv_v[r]) + dec_near[r] * dec_v[r : r + 1].astype(F32)
        dec_att.append(jnp.sum(jnp.where(vrow == vcol, att, 0.0), axis=0, keepdims=True))
    dec_rows = jnp.concatenate(dec_att, axis=0) if drows > 1 else dec_att[0]
    dec_ho = head_norm(jnp.broadcast_to(dec_rows, (group, heads * vw)) if drows == 1 else dec_rows)
    for c in wo_copies:
        c.wait()
    d_sends = [to_tp(d_send, d_recv, ds_sem, dr_sem, d) for d in range(1, tp)]
    for d in range(1, tp):
        d_send[d] = out_project(dec_ho, d)[0:drows]
        d_sends[d - 1].start()
    dec_own = out_project(dec_ho, 0)[0:drows]

    cv_copy.wait()
    for c in st_sends:
        c.wait_recv()

    def value_block(b):
        st = st_all[:, :, pl.ds(pl.multiple_of(b * LANES, LANES), LANES)]
        mx = st[:, 0:nstat]
        top = jnp.max(mx, axis=0)
        den = jnp.sum(st[:, nstat : 2 * nstat] * jnp.exp2((mx - top[None]) * C_EXP), axis=0)
        mine = st_all[me, 0:nstat, pl.ds(pl.multiple_of(b * LANES, LANES), LANES)]
        fac = jnp.exp2((mine - top) * C_EXP) / den
        fac = jnp.concatenate([fac, jnp.zeros((LANES - nstat, LANES), F32)], axis=0).T
        rs = pl.ds(b * LANES, LANES)
        for h in range(heads):
            f1 = fac[:, 2 * h : 2 * h + 1]
            f2 = fac[:, 2 * h + 1 : 2 * h + 2] * mix_lambda[h]
            wt = (e_v[2 * h, rs] * f1 - e_v[2 * h + 1, rs] * f2).astype(BF16)
            hv = slice(h * vw, (h + 1) * vw)
            att = dot(wt[:, 0:ctx], cv_v[:, hv]) + dot(wt[:, ctx:], vown[:, hv])
            att_send[pl.ds(b * (LANES // rows), LANES // rows), :, hv] = att.astype(BF16).reshape(
                LANES // rows, rows, vw
            )

    each_block(value_block)
    a_sends = []
    for d in range(1, kv):
        a_sends.append(
            to_kv(att_send.at[lax.rem(me + d, kv)], att_recv.at[me], as_sem, ar_sem, d)
        )
        a_sends[-1].start()
    total_att = att_send[me].astype(F32)
    for d, c in enumerate(a_sends, 1):
        c.wait_recv()
        total_att = total_att + att_recv[lax.rem(me - d + kv, kv)].astype(F32)

    ho = head_norm(total_att)
    p_sends = [to_tp(p_send, p_recv, ps_sem, pr_sem, d) for d in range(1, tp)]
    for d in range(1, tp):
        p_send[d] = out_project(ho, d)
        p_sends[d - 1].start()
    own = out_project(ho, 0).astype(F32)
    dsum = dec_own.astype(F32)
    for d in range(1, tp):
        d_sends[d - 1].wait_recv()
        dsum = dsum + d_recv[d].astype(F32)
    dec_out[...] = dsum.astype(BF16)
    for d in range(1, tp):
        p_sends[d - 1].wait_recv()
        own = own + p_recv[d].astype(F32)
    piece_out[...] = own.astype(BF16)
    for c in q_sends + st_sends + a_sends + d_sends + p_sends:
        c.wait_send()


def body(
    tokens, dec_tokens, norm_gain, w_query, w_key, w_value, w_out, head_gain, mix_lambda,
    ctx_keys, ctx_values, dec_keys, dec_values, dec_len, *, kv, tp,
):
    rows, width = tokens.shape
    drows = dec_tokens.shape[0]
    w = w_query.shape[2]
    heads = w // DH
    vwid = w_value.shape[1]
    ctx = ctx_keys.shape[1]
    slots = dec_keys.shape[2]
    total = rows * kv
    cols = w_out.shape[1] // tp
    padded = rows + -(-drows // 16) * 16
    srows = -(-4 * heads // 8) * 8
    any_spec = pl.BlockSpec(memory_space=pl.ANY)
    smem = pl.BlockSpec(memory_space=pltpu.SMEM)
    vmem = pl.BlockSpec(memory_space=pltpu.VMEM)
    dma = pltpu.SemaphoreType.DMA
    V = pltpu.VMEM
    return pl.pallas_call(
        functools.partial(kernel, kv, tp),
        out_shape=(
            jax.ShapeDtypeStruct((rows, cols), BF16),
            jax.ShapeDtypeStruct((drows, cols), BF16),
        ),
        in_specs=[any_spec] * 8 + [smem] * 2 + [any_spec] * 4,
        out_specs=(vmem, vmem),
        scratch_shapes=[
            V((rows, width), BF16), V((drows, width), BF16), V((1, width), F32),
            V((1, 2 * DH), F32),
            V((2, width, w), BF16), V((2, width, w), BF16), V((width, vwid), BF16),
            V((tp, vwid, cols), BF16),
            V((2, ctx, w), BF16), V((ctx, vwid), BF16),
            V((2, drows, slots, w), BF16), V((drows, slots, vwid), BF16),
            V((padded, width), BF16), V((kv, rows, 2 * w), BF16),
            V((2, LANES, w), BF16), V((LANES, vwid), BF16),
            V((2 * heads, total, ctx + LANES), F32),
            V((kv, srows, total), F32),
            V((kv, rows, vwid), BF16), V((kv, rows, vwid), BF16),
            V((tp, rows, cols), BF16), V((tp, rows, cols), BF16),
            V((tp, drows, cols), BF16), V((tp, drows, cols), BF16),
            dma((4,)), dma((4,)), dma((4,)), dma((4,)), dma((tp,)), dma((3,)), dma((3,)),
            dma((kv,)), dma((kv,)), dma((kv,)), dma((kv,)), dma((kv,)), dma((kv,)),
            dma((tp,)), dma((tp,)), dma((tp,)), dma((tp,)),
        ],
        compiler_params=pltpu.CompilerParams(
            collective_id=0, has_side_effects=True, vmem_limit_bytes=60 * 1024 * 1024
        ),
    )(
        tokens, dec_tokens, norm_gain.reshape(1, width), w_query, w_key, w_value, w_out,
        head_gain.reshape(1, 2 * DH), mix_lambda, dec_len, ctx_keys, ctx_values, dec_keys,
        dec_values,
    )


def solution(mesh):
    in_specs = (
        P("kv", None),
        P("kv", None),
        P(),
        P(None, None, "tp"),
        P(None, None, "tp"),
        P(None, "tp"),
        P("tp", None),
        P(),
        P("tp"),
        P(None, "kv", "tp"),
        P("kv", "tp"),
        P(None, "kv", None, "tp"),
        P("kv", None, "tp"),
        P("kv"),
    )
    out_specs = (P("kv", "tp"), P("kv", "tp"))
    step = functools.partial(body, kv=mesh.shape["kv"], tp=mesh.shape["tp"])
    return jax.shard_map(step, mesh=mesh, in_specs=in_specs, out_specs=out_specs, check_vma=False)
```

time: 191 us -> 34.8 us (0.18)
  waiting for transfers between devices: 72.5 us -> 0 us
  blocking collectives: 70.8 us -> 0 us
  Pallas kernels: 0 us -> 30.7 us
  matrix products: 17.9 us -> 0 us
  between operations: 15 us -> 1.29 us
  local copies, waits for them, and re-layouts: 9.9 us -> 2.65 us
  other arithmetic: 3.85 us -> 0 us
    reduce_scatter x2 -> x0, waiting for transfers between devices: 72.4 us -> none  [the longest x1 53.5 us: body(): lax.psum_scatter(terms.reshape(total_rows, terms.shape[2]), 'kv', scatter...]
    all_gather x1 -> x0, blocking collectives: 32.3 us -> none  [body(): gathered = lax.all_gather(query[:piece_rows], 'kv', axis=0, tiled=True)]
    pallas_call x0 -> x1, Pallas kernels: none -> 30.7 us  [body(): pl.pallas_call(functools.partial(kernel, kv, tp), out_shape=(jax.ShapeDty...]
    pmax x1 -> x0, blocking collectives: 21.4 us -> none  [body(): row_top = lax.pmax(local_max, 'kv')]
    dot_general x18 -> x0, matrix products: 17.9 us -> none  [the longest x1 3.55 us: body(): jnp.dot(heads_out, w_out, preferred_element_type=jnp.float32)]
    psum x1 -> x0, blocking collectives: 17.1 us -> none  [body(): row_sum = lax.psum(local_tot * jnp.exp(local_max - row_top), 'kv')]
    another operation x4 -> x0, local copies, waits for them, and re-layouts: 5.52 us -> none
    slice x6 -> x0, local copies, waits for them, and re-layouts: 3.32 us -> none  [the longest x2 2.69 us: body(): return (summed[:piece_rows], summed[piece_rows:])]
  transfers between devices with their start and end apart: 2 -> 0, of which waited for: 2 -> 0; matrix products, arithmetic and copies ran while one was open for 4% -> 0% of each run, Pallas kernels for 0% -> 0%
where the time goes in v1:
time: 34.8 us; the launch traced here: 34.6 us
  Pallas kernels  30.7 us (88%)
  local copies, waits for them, and re-layouts  2.65 us (8%)
  between operations  1.29 us (4%)
    pallas_call x1, Pallas kernels, body(): pl.pallas_call(functools.partial(kernel, kv, tp), out_shape=(jax.ShapeDty...  30.7 us
    unnamed x2, local copies, waits for them, and re-layouts  2.65 us

profile of v1, /device:TPU:0, one launch (start us, length us, event | category | flops | bytes accessed | tf_op | source)
XLA Modules:
  0.0 34.6 jit_solution(11177467263315618241)
XLA Ops:
  1.3 30.7 %shard_map.149 = (bf16[16,1024]{1,0:T(8,128)(2,1)}, bf16[1,1024]{1,0:T(2,128)(2,1)}) custom-call(bf16[16,4096]{1,0:T(8,128)(2,1)} %tokens.1, bf16[1,4096]{1,0:T(2,128)(2,1)} %dec_tokens.1, f32[1,4096]{1,0:T(1,128)} %bitcast.2, bf16[2,4096,256]{2,1,0:T(8,128)(2,1)} %w_query.1, bf16[2,4096,256]{2,1,0:T(8,128)(2,1)} %w_key.1, bf16[4096,512]{1,0:T(8,128)(2,1)} %w_value.1, ...), custom_call_target="tpu_custom_call" | custom-call | tf_op jit(solution)/shard_map/pallas_call | solution.py:360
  31.9 1.4 %copy.19 = bf16[16,1024]{1,0:T(8,128)(2,1)} copy(bf16[16,1024]{1,0:T(8,128)(2,1)} %get-tuple-element.4) | data formatting | bytes 65536
  33.3 1.3 %copy.20 = bf16[1,1024]{1,0:T(2,128)(2,1)} copy(bf16[1,1024]{1,0:T(2,128)(2,1)} %get-tuple-element.5) | data formatting | bytes 4096

commit v2 on v1

v2 whole, which is shorter than its diff:
```python
import functools
import math

import jax
import jax.numpy as jnp
from jax import lax
from jax.experimental import pallas as pl
from jax.experimental.pallas import tpu as pltpu
from jax.sharding import PartitionSpec as P

DH = 128
epsilon = 1e-06
MESH = pl.DeviceIdType.MESH
F32 = jnp.float32
BF16 = jnp.bfloat16
LANES = 128
C_EXP = DH ** (-0.5) * math.log2(math.e)


def dot(a, b):
    return jnp.dot(a, b, preferred_element_type=F32)


def dot_nt(a, b):
    return lax.dot_general(a, b, (((1,), (1,)), ((), ())), preferred_element_type=F32)


def kernel(
    kv, tp,
    tokens, dec_tokens, norm_gain, w_query, w_key, w_value, w_out, head_gain,
    mix_lambda, dec_len, ctx_keys, ctx_values, dec_keys, dec_values,
    out,
    lam_s, len_s, tok_v, dtok_v, gain_v, hgain_v, wq_v, wk_v, wv_v, wo_v,
    ck_v, cv_v, dk_v, dv_v,
    xs, q_all, kown, vown, st_send, st_recv, att_send, att_recv, p_send, p_recv, d_send, d_recv,
    sem_small, sem_q, sem_k, sem_v, sem_o, sem_c, sem_d,
    qs_sem, qr_sem, ss_sem, sr_sem, as_sem, ar_sem, ps_sem, pr_sem, ds_sem, dr_sem,
):
    me = lax.axis_index("kv")
    mt = lax.axis_index("tp")
    rows, width = tokens.shape
    drows = dec_tokens.shape[0]
    w = w_query.shape[2]
    heads = w // DH
    ctx = ctx_keys.shape[1]
    slots = dec_keys.shape[2]
    total = rows * kv
    cols = w_out.shape[1] // tp
    blocks = total // LANES
    padded = xs.shape[0]

    def tp_peer(d):
        chip = lax.rem(mt // 2 + d // 2, tp // 2)
        return chip * 2 + lax.rem(mt + d, 2)

    barrier = pltpu.get_barrier_semaphore()
    for d in range(1, kv):
        pl.semaphore_signal(
            barrier, inc=1, device_id=(lax.rem(me + d, kv), mt), device_id_type=MESH
        )
    for d in range(1, tp):
        pl.semaphore_signal(
            barrier, inc=1, device_id=(me, tp_peer(d)), device_id_type=MESH
        )

    small = [
        pltpu.make_async_copy(tokens, tok_v, sem_small.at[0]),
        pltpu.make_async_copy(dec_tokens, dtok_v, sem_small.at[1]),
        pltpu.make_async_copy(norm_gain, gain_v, sem_small.at[2]),
        pltpu.make_async_copy(head_gain, hgain_v, sem_small.at[3]),
        pltpu.make_async_copy(mix_lambda, lam_s, sem_small.at[4]),
        pltpu.make_async_copy(dec_len, len_s, sem_small.at[5]),
    ]
    for c in small:
        c.start()

    def weight_copies(src, dst, sem, parts):
        step = width // parts
        out = []
        for c in range(2):
            row = []
            for i in range(parts):
                sl = pl.ds(i * step, step)
                row.append(
                    pltpu.make_async_copy(src.at[c, sl], dst.at[c, sl], sem.at[c * parts + i])
                )
            out.append(row)
        return out

    parts = 2
    q_copies = weight_copies(w_query, wq_v, sem_q, parts)
    k_copies = weight_copies(w_key, wk_v, sem_k, parts)
    vstep = width // 4
    v_copies = [
        pltpu.make_async_copy(
            w_value.at[pl.ds(i * vstep, vstep)], wv_v.at[pl.ds(i * vstep, vstep)], sem_v.at[i]
        )
        for i in range(4)
    ]
    ck_copies = [pltpu.make_async_copy(ctx_keys.at[c], ck_v.at[c], sem_c.at[c]) for c in range(2)]
    cv_copy = pltpu.make_async_copy(ctx_values, cv_v, sem_c.at[2])
    dk_copies = [pltpu.make_async_copy(dec_keys.at[c], dk_v.at[c], sem_d.at[c]) for c in range(2)]
    dv_copy = pltpu.make_async_copy(dec_values, dv_v, sem_d.at[2])
    wo_copies = []
    for d in range(tp):
        start = pl.multiple_of(tp_peer(d) * cols, LANES)
        wo_copies.append(
            pltpu.make_async_copy(w_out.at[:, pl.ds(start, cols)], wo_v.at[d], sem_o.at[d])
        )
    for row in q_copies + k_copies:
        for c in row:
            c.start()
    for c in v_copies + ck_copies + [cv_copy] + dk_copies + [dv_copy] + wo_copies:
        c.start()

    kown[...] = jnp.zeros_like(kown)
    vown[...] = jnp.zeros_like(vown)
    xs[rows:, :] = jnp.zeros((padded - rows, width), BF16)
    for c in small:
        c.wait()
    gain = gain_v[...]

    def normed(x):
        xf = x.astype(F32)
        inv = lax.rsqrt(jnp.mean(xf * xf, axis=-1, keepdims=True) + epsilon)
        return (xf * inv * gain).astype(BF16)

    xs[0:rows, :] = normed(tok_v[...])
    xs[rows : rows + drows, :] = normed(dtok_v[...])

    def project(copies, weights, c):
        step = width // parts
        acc = None
        for i in range(parts):
            copies[c][i].wait()
            term = dot(xs[:, i * step : (i + 1) * step], weights[c, i * step : (i + 1) * step, :])
            acc = term if acc is None else acc + term
        return acc.astype(BF16)

    dec_q = []
    for c in range(2):
        qc = project(q_copies, wq_v, c)
        q_all[me, :, c * w : (c + 1) * w] = qc[0:rows]
        dec_q.append(qc[rows:])
    pl.semaphore_wait(barrier, kv + tp - 2)

    def to_kv(src, dst, send, recv, d):
        return pltpu.make_async_remote_copy(
            src_ref=src, dst_ref=dst, send_sem=send.at[d], recv_sem=recv.at[d],
            device_id=(lax.rem(me + d, kv), mt), device_id_type=MESH,
        )

    q_sends = [to_kv(q_all.at[me], q_all.at[me], qs_sem, qr_sem, d) for d in range(1, kv)]
    for c in q_sends:
        c.start()

    dec_k = []
    for c in range(2):
        kc = project(k_copies, wk_v, c)
        kown[c, 0:rows, :] = kc[0:rows]
        dec_k.append(kc[rows:])
    acc = None
    for i in range(4):
        v_copies[i].wait()
        term = dot(xs[:, i * vstep : (i + 1) * vstep], wv_v[i * vstep : (i + 1) * vstep, :])
        acc = term if acc is None else acc + term
    vc = acc.astype(BF16)
    vown[0:rows, :] = vc[0:rows]
    dec_v = vc[rows:]

    for c in ck_copies:
        c.wait()
    cv_copy.wait()
    for c in q_sends:
        c.wait_recv()
    vw = 2 * DH
    nstat = 2 * heads
    per = LANES // rows

    def head_block(h, b):
        slots_b = pl.ds(b * per, per)
        qb = q_all[slots_b].reshape(LANES, 2 * w)
        pos = b * LANES + lax.broadcasted_iota(jnp.int32, (LANES, LANES), 0)
        lane = lax.broadcasted_iota(jnp.int32, (LANES, LANES), 1)
        ok = (lane < rows) & (lane + me * rows <= pos)
        if h == 0:
            stats = jnp.zeros((LANES, LANES), F32)
        else:
            stats = st_send[slots_b].reshape(LANES, LANES)
        hs = slice(h * DH, (h + 1) * DH)
        hv = slice(h * vw, (h + 1) * vw)
        for c in range(2):
            q = qb[:, c * w + h * DH : c * w + (h + 1) * DH]
            far = dot_nt(q, ck_v[c, :, hs])
            near = dot_nt(q, kown[c, :, hs])
            near = jnp.where(ok, near, -jnp.inf)
            top = jnp.maximum(
                jnp.max(far, axis=-1, keepdims=True), jnp.max(near, axis=-1, keepdims=True)
            )
            ef = jnp.exp2((far - top) * C_EXP)
            en = jnp.exp2((near - top) * C_EXP)
            tot = jnp.sum(ef, axis=-1, keepdims=True) + jnp.sum(en, axis=-1, keepdims=True)
            att = dot(ef.astype(BF16), cv_v[:, hv]) + dot(en.astype(BF16), vown[:, hv])
            att_send[h, slots_b, :, c * vw : (c + 1) * vw] = att.astype(BF16).reshape(
                per, rows, vw
            )
            i = 2 * h + c
            stats = jnp.where(lane == i, top, stats)
            stats = jnp.where(lane == nstat + i, tot, stats)
        st_send[slots_b] = stats.reshape(per, rows, LANES)

    a_sends = []
    for h in range(heads):
        if blocks == 1:
            head_block(h, 0)
        else:
            pl.loop(0, blocks)(functools.partial(head_block, h))
        if h == heads - 1:
            st_sends = []
            for d in range(1, kv):
                peer = lax.rem(me + d, kv)
                st_sends.append(to_kv(st_send.at[peer], st_recv.at[me], ss_sem, sr_sem, d))
                st_sends[-1].start()
        a_sends.append([])
        for d in range(1, kv):
            peer = lax.rem(me + d, kv)
            a_sends[h].append(
                to_kv(att_send.at[h, peer], att_recv.at[h, me], as_sem.at[h], ar_sem.at[h], d)
            )
            a_sends[h][-1].start()

    hgain = hgain_v[...]
    group = 16
    hrow = lax.broadcasted_iota(jnp.int32, (group, w), 0)
    hcol = lax.broadcasted_iota(jnp.int32, (group, w), 1) // DH
    own_head = hrow == hcol
    row1 = lax.broadcasted_iota(jnp.int32, (group, 1), 0)
    lam_col = jnp.zeros((group, 1), F32)
    for h in range(heads):
        lam_col = jnp.where(row1 == h, lam_s[h], lam_col)
    for c in dk_copies:
        c.wait()
    slot_id = lax.broadcasted_iota(jnp.int32, (group, slots), 1)
    vrow = lax.broadcasted_iota(jnp.int32, (group, heads * vw), 0)
    vcol = lax.broadcasted_iota(jnp.int32, (group, heads * vw), 1) // vw
    dec_att = []
    for r in range(drows):
        far_p = []
        near_p = []
        for c in range(2):
            qr = jnp.broadcast_to(dec_q[c][r : r + 1].astype(F32), (group, w))
            qr = jnp.where(own_head, qr, 0.0)
            kr = dec_k[c][r : r + 1].astype(F32)
            near = jnp.sum(qr * kr, axis=-1, keepdims=True)
            far = dot_nt(qr.astype(BF16), dk_v[c, r])
            far = jnp.where(slot_id < len_s[r], far, -jnp.inf)
            top = jnp.maximum(jnp.max(far, axis=-1, keepdims=True), near)
            ef = jnp.exp2((far - top) * C_EXP)
            en = jnp.exp2((near - top) * C_EXP)
            den = jnp.sum(ef, axis=-1, keepdims=True) + en
            far_p.append(ef / den)
            near_p.append(en / den)
        far_w = (far_p[0] - lam_col * far_p[1]).astype(BF16)
        near_w = (near_p[0] - lam_col * near_p[1]).astype(BF16).astype(F32)
        if r == 0:
            dv_copy.wait()
        att = dot(far_w, dv_v[r]) + near_w * dec_v[r : r + 1].astype(F32)
        dec_att.append(jnp.sum(jnp.where(vrow == vcol, att, 0.0), axis=0, keepdims=True))

    def head_norm(att, h):
        inv = lax.rsqrt(jnp.mean(att * att, axis=-1, keepdims=True) + epsilon)
        return (att * inv * hgain).astype(BF16)

    def out_project(ho, d):
        acc = None
        for h in range(heads):
            term = dot(ho[h], wo_v[d, h * vw : (h + 1) * vw, :])
            acc = term if acc is None else acc + term
        return acc.astype(BF16)

    def to_tp(src, dst, send, recv, d):
        return pltpu.make_async_remote_copy(
            src_ref=src.at[d], dst_ref=dst.at[d], send_sem=send.at[d], recv_sem=recv.at[d],
            device_id=(me, tp_peer(d)), device_id_type=MESH,
        )

    dec_rows = jnp.concatenate(dec_att, axis=0) if drows > 1 else dec_att[0]
    dec_rows = dec_rows if drows > 1 else jnp.broadcast_to(dec_rows, (group, heads * vw))
    dec_ho = [head_norm(dec_rows[:, h * vw : (h + 1) * vw], h) for h in range(heads)]
    for c in wo_copies:
        c.wait()
    order = list(range(tp - 1, 0, -1))
    d_sends = {d: to_tp(d_send, d_recv, ds_sem, dr_sem, d) for d in order}
    for d in order:
        d_send[d] = out_project(dec_ho, d)[0:drows]
        d_sends[d].start()
    dec_own = out_project(dec_ho, 0)[0:drows]

    for c in st_sends:
        c.wait_recv()
    lane = lax.broadcasted_iota(jnp.int32, (rows, LANES), 1)
    sts = {0: st_send[me]}
    for d in range(1, kv):
        sts[d] = st_recv[lax.rem(me - d + kv, kv)]
    top = sts[0]
    for d in range(1, kv):
        top = jnp.maximum(top, sts[d])
    den = jnp.zeros((rows, LANES), F32)
    fac = {}
    for d in range(kv):
        fac[d] = jnp.exp2((sts[d] - top) * C_EXP)
        den = den + fac[d] * pltpu.roll(sts[d], LANES - nstat, 1)
    den = jnp.where(lane < nstat, den, 1.0)
    part = jnp.ones((rows, LANES), F32)
    for h in range(heads):
        part = jnp.where(lane == 2 * h + 1, -lam_s[h], part)
    part = part / den
    for d in range(kv):
        fac[d] = fac[d] * part
    ho = []
    for h in range(heads):
        total_att = None
        for d in range(kv):
            if d == 0:
                blk = att_send[h, me]
            else:
                a_sends[h][d - 1].wait_recv()
                blk = att_recv[h, lax.rem(me - d + kv, kv)]
            for c in range(2):
                i = 2 * h + c
                term = fac[d][:, i : i + 1] * blk[:, c * vw : (c + 1) * vw].astype(F32)
                total_att = term if total_att is None else total_att + term
        ho.append(head_norm(total_att, h))

    p_sends = {d: to_tp(p_send, p_recv, ps_sem, pr_sem, d) for d in order}
    for d in order:
        p_send[d] = out_project(ho, d)
        p_sends[d].start()
    own = out_project(ho, 0).astype(F32)
    dsum = dec_own.astype(F32)
    for d in order:
        d_sends[d].wait_recv()
        dsum = dsum + d_recv[d].astype(F32)
    out[rows:, :] = jnp.broadcast_to(dsum, (out.shape[0] - rows, cols)).astype(BF16) if (
        drows == 1
    ) else jnp.concatenate(
        [dsum, jnp.zeros((out.shape[0] - rows - drows, cols), F32)], axis=0
    ).astype(BF16)
    for d in order:
        p_sends[d].wait_recv()
        own = own + p_recv[d].astype(F32)
    out[0:rows, :] = own.astype(BF16)
    for c in q_sends + st_sends + [c for row in a_sends for c in row]:
        c.wait_send()
    for d in order:
        d_sends[d].wait_send()
        p_sends[d].wait_send()


def body(
    tokens, dec_tokens, norm_gain, w_query, w_key, w_value, w_out, head_gain, mix_lambda,
    ctx_keys, ctx_values, dec_keys, dec_values, dec_len, *, kv, tp,
):
    rows, width = tokens.shape
    drows = dec_tokens.shape[0]
    w = w_query.shape[2]
    heads = w // DH
    vwid = w_value.shape[1]
    ctx = ctx_keys.shape[1]
    slots = dec_keys.shape[2]
    cols = w_out.shape[1] // tp
    padded = rows + -(-drows // 16) * 16
    any_spec = pl.BlockSpec(memory_space=pltpu.HBM)
    vmem = pl.BlockSpec(memory_space=pltpu.VMEM)
    dma = pltpu.SemaphoreType.DMA
    V = pltpu.VMEM
    out = pl.pallas_call(
        functools.partial(kernel, kv, tp),
        out_shape=jax.ShapeDtypeStruct((padded, cols), BF16),
        in_specs=[any_spec] * 14,
        out_specs=vmem,
        scratch_shapes=[
            pltpu.SMEM((heads,), F32), pltpu.SMEM((drows,), jnp.int32),
            V((rows, width), BF16), V((drows, width), BF16), V((1, width), F32),
            V((1, 2 * DH), F32),
            V((2, width, w), BF16), V((2, width, w), BF16), V((width, vwid), BF16),
            V((tp, vwid, cols), BF16),
            V((2, ctx, w), BF16), V((ctx, vwid), BF16),
            V((2, drows, slots, w), BF16), V((drows, slots, vwid), BF16),
            V((padded, width), BF16), V((kv, rows, 2 * w), BF16),
            V((2, LANES, w), BF16), V((LANES, vwid), BF16),
            V((kv, rows, LANES), F32), V((kv, rows, LANES), F32),
            V((heads, kv, rows, 4 * DH), BF16), V((heads, kv, rows, 4 * DH), BF16),
            V((tp, rows, cols), BF16), V((tp, rows, cols), BF16),
            V((tp, drows, cols), BF16), V((tp, drows, cols), BF16),
            dma((6,)), dma((4,)), dma((4,)), dma((4,)), dma((tp,)), dma((3,)), dma((3,)),
            dma((kv,)), dma((kv,)), dma((kv,)), dma((kv,)), dma((heads, kv)), dma((heads, kv)),
            dma((tp,)), dma((tp,)), dma((tp,)), dma((tp,)),
        ],
        compiler_params=pltpu.CompilerParams(
            collective_id=0, has_side_effects=True, vmem_limit_bytes=60 * 1024 * 1024
        ),
    )(
        tokens, dec_tokens, norm_gain.reshape(1, width), w_query, w_key, w_value, w_out,
        head_gain.reshape(1, 2 * DH), mix_lambda, dec_len, ctx_keys, ctx_values, dec_keys,
        dec_values,
    )
    return out[:rows], out[rows : rows + drows]


def solution(mesh):
    in_specs = (
        P("kv", None),
        P("kv", None),
        P(),
        P(None, None, "tp"),
        P(None, None, "tp"),
        P(None, "tp"),
        P("tp", None),
        P(),
        P("tp"),
        P(None, "kv", "tp"),
        P("kv", "tp"),
        P(None, "kv", None, "tp"),
        P("kv", None, "tp"),
        P("kv"),
    )
    out_specs = (P("kv", "tp"), P("kv", "tp"))
    step = functools.partial(body, kv=mesh.shape["kv"], tp=mesh.shape["tp"])
    return jax.shard_map(step, mesh=mesh, in_specs=in_specs, out_specs=out_specs, check_vma=False)
```

time: 34.8 us -> 34.4 us (0.989)
  Pallas kernels: 30.7 us -> 30.1 us
    slice x0 -> x2, local copies, waits for them, and re-layouts: none -> 2.69 us  [body(): return (out[:rows], out[rows:rows + drows])]
    unnamed x2 -> x0, local copies, waits for them, and re-layouts: 2.65 us -> none
    pallas_call x1, Pallas kernels: 30.7 us -> 30.1 us  [body(): pl.pallas_call(functools.partial(kernel, kv, tp), out_shape=jax.ShapeDtyp...]
where the time goes in v2:
time: 34.4 us; the launch traced here: 34.1 us
  Pallas kernels  30.1 us (88%)
  local copies, waits for them, and re-layouts  2.69 us (8%)
  between operations  1.29 us (4%)
    pallas_call x1, Pallas kernels, body(): pl.pallas_call(functools.partial(kernel, kv, tp), out_shape=jax.ShapeDtyp...  30.1 us
    slice x2, local copies, waits for them, and re-layouts, body(): return (out[:rows], out[rows:rows + drows])  2.69 us

profile of v2, /device:TPU:0, one launch (start us, length us, event | category | flops | bytes accessed | tf_op | source)
XLA Modules:
  0.0 34.1 jit_solution(262283937633553698)
XLA Ops:
  1.3 30.1 %shard_map.149 = bf16[32,1024]{1,0:T(8,128)(2,1)} custom-call(bf16[16,4096]{1,0:T(8,128)(2,1)} %tokens.1, bf16[1,4096]{1,0:T(2,128)(2,1)} %dec_tokens.1, f32[1,4096]{1,0:T(1,128)} %bitcast.2, bf16[2,4096,256]{2,1,0:T(8,128)(2,1)} %w_query.1, bf16[2,4096,256]{2,1,0:T(8,128)(2,1)} %w_key.1, bf16[4096,512]{1,0:T(8,128)(2,1)} %w_value.1, ...), custom_call_target="tpu_custom_call" | custom-call | tf_op jit(solution)/shard_map/pallas_call | solution.py:377
  31.4 1.3 %slice.7 = bf16[1,1024]{1,0:T(2,128)(2,1)} slice(bf16[32,1024]{1,0:T(8,128)(2,1)} %shard_map.149), slice={[16:17], [0:1024]} | slice | bytes 4096 | tf_op jit(solution)/shard_map/slice | solution.py:408
  32.7 1.4 %slice.6 = bf16[16,1024]{1,0:T(8,128)(2,1)} slice(bf16[32,1024]{1,0:T(8,128)(2,1)} %shard_map.149), slice={[0:16], [0:1024]} | slice | bytes 65536 | tf_op jit(solution)/shard_map/slice | solution.py:408

commit v3 on v2

--- a/solution.py
+++ b/solution.py
@@ -107,11 +107,21 @@
         wo_copies.append(
             pltpu.make_async_copy(w_out.at[:, pl.ds(start, cols)], wo_v.at[d], sem_o.at[d])
         )
-    for row in q_copies + k_copies:
-        for c in row:
+    k_flat = [c for row in k_copies for c in row]
+    stages = [
+        [c for row in q_copies for c in row],
+        k_flat,
+        v_copies,
+        ck_copies + [cv_copy],
+        dk_copies + [dv_copy],
+        wo_copies,
+    ]
+
+    def start_stage(i):
+        for c in stages[i]:
             c.start()
-    for c in v_copies + ck_copies + [cv_copy] + dk_copies + [dv_copy] + wo_copies:
-        c.start()
+
+    start_stage(0)
 
     kown[...] = jnp.zeros_like(kown)
     vown[...] = jnp.zeros_like(vown)
@@ -142,6 +152,9 @@
         qc = project(q_copies, wq_v, c)
         q_all[me, :, c * w : (c + 1) * w] = qc[0:rows]
         dec_q.append(qc[rows:])
+        start_stage(1 + c)
+        if c == 1:
+            start_stage(3)
     pl.semaphore_wait(barrier, kv + tp - 2)
 
     def to_kv(src, dst, send, recv, d):
@@ -150,7 +163,8 @@
             device_id=(lax.rem(me + d, kv), mt), device_id_type=MESH,
         )
 
-    q_sends = [to_kv(q_all.at[me], q_all.at[me], qs_sem, qr_sem, d) for d in range(1, kv)]
+    far_first = sorted(range(1, kv), key=lambda d: (-min(d, kv - d), d))
+    q_sends = [to_kv(q_all.at[me], q_all.at[me], qs_sem, qr_sem, d) for d in far_first]
     for c in q_sends:
         c.start()
 
@@ -159,6 +173,7 @@
         kc = project(k_copies, wk_v, c)
         kown[c, 0:rows, :] = kc[0:rows]
         dec_k.append(kc[rows:])
+        start_stage(4 + c)
     acc = None
     for i in range(4):
         v_copies[i].wait()
@@ -217,17 +232,17 @@
             pl.loop(0, blocks)(functools.partial(head_block, h))
         if h == heads - 1:
             st_sends = []
-            for d in range(1, kv):
+            for d in far_first:
                 peer = lax.rem(me + d, kv)
                 st_sends.append(to_kv(st_send.at[peer], st_recv.at[me], ss_sem, sr_sem, d))
                 st_sends[-1].start()
-        a_sends.append([])
-        for d in range(1, kv):
+        a_sends.append({})
+        for d in far_first:
             peer = lax.rem(me + d, kv)
-            a_sends[h].append(
-                to_kv(att_send.at[h, peer], att_recv.at[h, me], as_sem.at[h], ar_sem.at[h], d)
+            a_sends[h][d] = to_kv(
+                att_send.at[h, peer], att_recv.at[h, me], as_sem.at[h], ar_sem.at[h], d
             )
-            a_sends[h][-1].start()
+            a_sends[h][d].start()
 
     hgain = hgain_v[...]
     group = 16
@@ -324,7 +339,7 @@
             if d == 0:
                 blk = att_send[h, me]
             else:
-                a_sends[h][d - 1].wait_recv()
+                a_sends[h][d].wait_recv()
                 blk = att_recv[h, lax.rem(me - d + kv, kv)]
             for c in range(2):
                 i = 2 * h + c
@@ -350,7 +365,7 @@
         p_sends[d].wait_recv()
         own = own + p_recv[d].astype(F32)
     out[0:rows, :] = own.astype(BF16)
-    for c in q_sends + st_sends + [c for row in a_sends for c in row]:
+    for c in q_sends + st_sends + [c for row in a_sends for c in row.values()]:
         c.wait_send()
     for d in order:
         d_sends[d].wait_send()
@@ -405,7 +420,19 @@
         head_gain.reshape(1, 2 * DH), mix_lambda, dec_len, ctx_keys, ctx_values, dec_keys,
         dec_values,
     )
-    return out[:rows], out[rows : rows + drows]
+    def split(src, piece_ref, dec_ref):
+        piece_ref[...] = src[0:rows, :]
+        dec_ref[...] = src[rows : rows + drows, :]
+
+    return pl.pallas_call(
+        split,
+        out_shape=(
+            jax.ShapeDtypeStruct((rows, cols), BF16),
+            jax.ShapeDtypeStruct((drows, cols), BF16),
+        ),
+        in_specs=[vmem],
+        out_specs=(vmem, vmem),
+    )(out)
 
 
 def solution(mesh):

time: 34.4 us -> 29.2 us (0.85)
  local copies, waits for them, and re-layouts: 2.69 us -> 0 us
  Pallas kernels: 30.1 us -> 27.8 us
    pallas_call x1, Pallas kernels: 30.1 us -> 26.3 us  [body(): pl.pallas_call(functools.partial(kernel, kv, tp), out_shape=jax.ShapeDtyp...]
    slice x2 -> x0, local copies, waits for them, and re-layouts: 2.69 us -> none  [body(): return (out[:rows], out[rows:rows + drows])]
    pallas_call x0 -> x1, Pallas kernels: none -> 1.46 us  [body(): pl.pallas_call(split, out_shape=(jax.ShapeDtypeStruct((rows, cols), BF16)...]
where the time goes in v3:
time: 29.2 us; the launch traced here: 29.1 us
  Pallas kernels  27.8 us (95%)
  between operations  1.29 us (4%)
    pallas_call x1, Pallas kernels, body(): pl.pallas_call(functools.partial(kernel, kv, tp), out_shape=jax.ShapeDtyp...  26.3 us
    pallas_call x1, Pallas kernels, body(): pl.pallas_call(split, out_shape=(jax.ShapeDtypeStruct((rows, cols), BF16)...  1.46 us

profile of v3, /device:TPU:0, one launch (start us, length us, event | category | flops | bytes accessed | tf_op | source)
XLA Modules:
  0.0 29.1 jit_solution(5396678087312868934)
XLA Ops:
  1.3 26.3 %shard_map.149.src = bf16[32,1024]{1,0:T(8,128)(2,1)} custom-call(bf16[16,4096]{1,0:T(8,128)(2,1)} %tokens.1, bf16[1,4096]{1,0:T(2,128)(2,1)} %dec_tokens.1, f32[1,4096]{1,0:T(1,128)} %bitcast.2, bf16[2,4096,256]{2,1,0:T(8,128)(2,1)} %w_query.1, bf16[2,4096,256]{2,1,0:T(8,128)(2,1)} %w_key.1, bf16[4096,512]{1,0:T(8,128)(2,1)} %w_value.1, ...), custom_call_target="tpu_custom_call" | custom-call | tf_op jit(solution)/shard_map/pallas_call | solution.py:392
  27.6 1.5 %shard_map.150 = (bf16[16,1024]{1,0:T(8,128)(2,1)}, bf16[1,1024]{1,0:T(2,128)(2,1)}) custom-call(bf16[32,1024]{1,0:T(8,128)(2,1)} %shard_map.149.src), custom_call_target="tpu_custom_call" | custom-call | tf_op jit(solution)/shard_map/pallas_call | solution.py:427
